TPU v7x, 32 devices: a whole 2x2x4 slice. The times are simulated.
32 devices in a mesh: ep: 8 (over z, y), tp: 4 (over x, core).
Axes of the slice: x: 2, y: 2, z: 4, core: 2. Of those that a mesh axis runs over, the one named last changes fastest.
Arguments:
- tokens: bfloat16 [64, 1024], P('ep'), may hold values from -6 to 6
- mix_gain: float32 [1024], replicated, may hold values from 0.1 to 1.9
- w_query: bfloat16 [1024, 512], P(None, 'tp'), may hold values from -0.1875 to 0.1875
- w_key: bfloat16 [1024, 512], P(None, 'tp'), may hold values from -0.1875 to 0.1875
- w_value: bfloat16 [1024, 1024], P(None, 'tp'), may hold values from -0.1875 to 0.1875
- w_ogate: bfloat16 [1024, 1024], P(None, 'tp'), may hold values from -0.1875 to 0.1875
- w_igate: bfloat16 [1024, 4], replicated, may hold values from -0.1875 to 0.1875
- w_fgate: bfloat16 [1024, 4], replicated, may hold values from -0.1875 to 0.1875
- forget_bias: float32 [4], replicated, may hold values from -1 to 3
- head_gain: float32 [1024], P('tp'), may hold values from 0.1 to 1.9
- w_out: bfloat16 [1024, 1024], P('tp'), may hold values from -0.1875 to 0.1875
- memory: float32 [64, 4, 128, 256], P('ep', 'tp'), may hold values from -0.4 to 0.4
- normalizer: float32 [64, 4, 128], P('ep', 'tp'), may hold values from -0.4 to 0.4
- running_max: float32 [64, 4], P('ep', 'tp'), may hold values from -4 to 4
- ffn_gain: float32 [1024], replicated, may hold values from 0.1 to 1.9
- route: int32 [64, 2], replicated, may hold values from 0 to 7, all different within a row; in each aligned block of 64 rows (0 to 63, 64 to 127, ...) at most 32 rows name the same one
- route_weight: float32 [64, 2], replicated, may hold values from 0.05 to 1
- w_gate: bfloat16 [8, 1024, 512], P('ep', None, 'tp'), may hold values from -0.1875 to 0.1875
- w_up: bfloat16 [8, 1024, 512], P('ep', None, 'tp'), may hold values from -0.1875 to 0.1875
- w_down: bfloat16 [8, 512, 1024], P('ep', 'tp'), may hold values from -0.25 to 0.25
Outputs:
- mixed: bfloat16 [64, 1024], P(None, 'ep')
- new_memory: float32 [64, 4, 128, 256], P('ep', 'tp')
- new_normalizer: float32 [64, 4, 128], P('ep', 'tp')
- new_max: float32 [64, 4], P('ep', 'tp')
Inputs may be any that keep to these rules, and one draw needn't show every extreme that they name: `route`: each expert is named by at most 32 routes in all, a bound that some block reaches; the two choices of a token differ.
All inputs are finite; a program needn't handle non-finite values.
Results may differ from a plain program's by a relative error of at most 0.014.
Values may be sent and summed in bfloat16 or wider, within the bound.
A program may use at most 64 MiB of HBM per device.

v0:
```python
import jax
import jax.numpy as jnp
from jax import lax
from jax.sharding import PartitionSpec as P

EXPERT_CAPACITY = 32


EPS = 1e-06


def round_trip(values):
    rounded = lax.optimization_barrier(values.astype(jnp.bfloat16))
    return rounded.astype(jnp.float32)


def norm_rows(values, gain):
    floats = values.astype(jnp.float32)
    scale = lax.rsqrt(jnp.mean(floats * floats, axis=-1, keepdims=True) + EPS)
    return (floats * scale * gain).astype(jnp.bfloat16)


def slot_targets(route, expert_count, capacity):
    flat = route.reshape(-1)
    onehot = (flat[:, None] == jnp.arange(expert_count, dtype=jnp.int32)[None, :]).astype(jnp.int32)
    before = jnp.cumsum(onehot, axis=0) - onehot
    slot = jnp.sum(before * onehot, axis=1)
    return flat * capacity + slot


def shards(
    tokens,
    mix_gain,
    w_query,
    w_key,
    w_value,
    w_ogate,
    w_igate,
    w_fgate,
    forget_bias,
    head_gain,
    w_out,
    memory,
    normalizer,
    running_max,
    ffn_gain,
    route,
    route_weight,
    w_gate,
    w_up,
    w_down,
):
    width = tokens.shape[1]
    col_count = width // lax.axis_size("ep")
    qk_dim = w_query.shape[1]
    normed = norm_rows(tokens, mix_gain)
    query = round_trip(jnp.dot(normed, w_query, preferred_element_type=jnp.float32))
    scaled_key = round_trip(
        jnp.dot(normed, w_key, preferred_element_type=jnp.float32)
    ) * qk_dim ** (-0.5)
    value = round_trip(jnp.dot(normed, w_value, preferred_element_type=jnp.float32))
    ogate = round_trip(jnp.dot(normed, w_ogate, preferred_element_type=jnp.float32))
    head_pick = (jnp.arange(w_igate.shape[1], dtype=jnp.int32) == lax.axis_index("tp")).astype(
        jnp.float32
    )
    log_in = jnp.sum(
        jnp.dot(normed, w_igate, preferred_element_type=jnp.float32) * head_pick, axis=1
    )
    forget_pre = jnp.sum(
        jnp.dot(normed, w_fgate, preferred_element_type=jnp.float32) * head_pick, axis=1
    )
    log_forget = jax.nn.log_sigmoid(forget_pre + jnp.sum(forget_bias * head_pick))
    old_max = running_max[:, 0]
    new_max = jnp.maximum(log_forget + old_max, log_in)
    keep = jnp.exp(log_forget + old_max - new_max)
    admit = jnp.exp(log_in - new_max)
    state = (
        keep[:, None, None] * memory[:, 0]
        + admit[:, None, None] * scaled_key[:, :, None] * value[:, None, :]
    )
    norm_state = keep[:, None] * normalizer[:, 0] + admit[:, None] * scaled_key
    numer = jnp.einsum("tk,tkv->tv", query, state, precision=lax.Precision.HIGHEST)
    denom = jnp.sum(query * norm_state, axis=1)
    read = numer / jnp.maximum(jnp.abs(denom), jnp.exp(-new_max))[:, None]
    scale = lax.rsqrt(jnp.mean(read * read, axis=-1, keepdims=True) + EPS)
    gated = (jax.nn.sigmoid(ogate) * read * scale * head_gain).astype(jnp.bfloat16)
    local_output = lax.psum(
        jnp.dot(gated, w_out, preferred_element_type=jnp.float32).astype(jnp.bfloat16), "tp"
    ).astype(jnp.float32)
    middle_rows = (tokens.astype(jnp.float32) + local_output).astype(jnp.bfloat16)
    middle = lax.all_to_all(middle_rows, "ep", split_axis=1, concat_axis=0, tiled=True)
    expert_count = w_gate.shape[0] * lax.axis_size("ep")
    topk_count = route.shape[1]
    targets = slot_targets(route, expert_count, EXPERT_CAPACITY)
    buffer = (
        jnp.zeros((expert_count * EXPERT_CAPACITY, col_count), jnp.bfloat16)
        .at[targets]
        .set(jnp.repeat(middle, topk_count, axis=0))
    )
    buffer = buffer.reshape(expert_count, EXPERT_CAPACITY, col_count)
    rows = lax.all_to_all(buffer, "ep", split_axis=0, concat_axis=2, tiled=True)
    rows = norm_rows(rows, ffn_gain)
    gate_v = jnp.einsum("ecd,edf->ecf", rows, w_gate, preferred_element_type=jnp.float32)
    up_v = jnp.einsum("ecd,edf->ecf", rows, w_up, preferred_element_type=jnp.float32)
    activation = (jax.nn.silu(gate_v) * up_v).astype(jnp.bfloat16)
    partial_value = jnp.einsum(
        "ecf,efd->ecd", activation, w_down, preferred_element_type=jnp.float32
    )
    results = lax.psum(partial_value.astype(jnp.bfloat16), "tp")
    returned = lax.all_to_all(results, "ep", split_axis=2, concat_axis=0, tiled=True)
    picked = returned.reshape(expert_count * EXPERT_CAPACITY, col_count)[targets]
    picked = picked.reshape(route.shape[0], topk_count, col_count).astype(jnp.float32)
    weights = route_weight / jnp.sum(route_weight, axis=1, keepdims=True)
    mixed = (middle.astype(jnp.float32) + jnp.sum(picked * weights[:, :, None], axis=1)).astype(
        jnp.bfloat16
    )
    return (mixed, state[:, None], norm_state[:, None], new_max[:, None])


def solution(mesh):
    return jax.shard_map(
        shards,
        mesh=mesh,
        in_specs=(
            P("ep", None),
            P(),
            P(None, "tp"),
            P(None, "tp"),
            P(None, "tp"),
            P(None, "tp"),
            P(),
            P(),
            P(),
            P("tp"),
            P("tp", None),
            P("ep", "tp", None, None),
            P("ep", "tp", None),
            P("ep", "tp"),
            P(),
            P(),
            P(),
            P("ep", None, "tp"),
            P("ep", None, "tp"),
            P("ep", "tp", None),
        ),
        out_specs=(P(None, "ep"), P("ep", "tp", None, None), P("ep", "tp", None), P("ep", "tp")),
        check_vma=False,
    )
```

profile of v0, /device:TPU:0, one launch (start us, length us, event | category | flops | bytes accessed | tf_op | source)
XLA Modules:
  0.0 114.8 jit_solution(4171381798939121330)
XLA Ops:
  7.2 1.4 %fusion.48 = f32[]{:T(128)} fusion(f32[4]{0:T(128)} %param.28, s32[]{:T(128)S(6)} %axis_index.12), kind=kLoop, calls=%fused_computation.81 | loop fusion | flops 11 | bytes 24 | tf_op jit(solution)/shard_map/reduce_sum | solution.py:72
  8.7 0.8 fusion.28
  9.5 0.9 fusion.3
  10.4 0.9 fusion.2
  11.3 1.3 %fusion.46 = (f32[8]{0:T(128)S(1)}, f32[8]{0:T(128)S(1)}) fusion(f32[8]{0:T(128)S(1)} %fusion.3, f32[8,1]{0,1:T(1,128)} %param.33, f32[8]{0:T(128)S(1)} %fusion.2, f32[]{:T(128)} %fusion.48), kind=kLoop, calls=%fused_computation.79 | loop fusion | flops 96 | bytes 164 | tf_op jit(solution)/shard_map/exp | solution.py:75
  12.7 1.3 %exponential_bitcast_fusion = (f32[8]{0:T(128)S(1)}, f32[8,1]{0,1:T(1,128)S(1)}) fusion(f32[8]{0:T(128)S(1)} %fusion.3, f32[8,1]{0,1:T(1,128)} %param.33, f32[8]{0:T(128)S(1)} %fusion.2, f32[]{:T(128)} %fusion.48), kind=kLoop, calls=%fused_computation.104 | loop fusion | flops 96 | bytes 164 | tf_op jit(solution)/shard_map/mul | solution.py:81
  14.1 0.9 convolution_convert_fusion.5
  14.9 1.2 %convolution_convert_fusion.4 = bf16[8,128]{1,0:T(8,128)(2,1)S(1)} fusion(bf16[1024,128]{1,0:T(8,128)(2,1)} %param.23, bf16[8,1024]{1,0:T(8,128)(2,1)S(1)} %copy-done.3, f32[1024]{0:T(1024)} %param.21, f32[8]{0:T(128)S(1)} %add_rsqrt_fusion.2), kind=kOutput, calls=%fused_computation.9 | convolution fusion | flops 2130944 | bytes 284704 | tf_op jit(solution)/shard_map/dot_general | solution.py:59
  16.1 0.9 convolution_convert_fusion.2
  17.0 1.3 %convolution_convert_fusion.3 = bf16[8,256]{1,0:T(8,128)(2,1)S(1)} fusion(bf16[1024,256]{1,0:T(8,128)(2,1)} %param.25, bf16[8,1024]{1,0:T(8,128)(2,1)S(1)} %copy-done.3, f32[1024]{0:T(1024)} %param.21, f32[8]{0:T(128)S(1)} %add_rsqrt_fusion.2), kind=kOutput, calls=%fused_computation.8 | convolution fusion | flops 4229120 | bytes 548896 | tf_op jit(solution)/shard_map/dot_general | solution.py:62
  18.3 0.7 copy-done.10
  19.0 0.8 multiply_reduce_fusion.1
  19.8 0.6 fusion.5
  20.6 0.7 copy-done.13
  21.5 12.7 %psum.14 = bf16[8,1024]{1,0:T(8,128)(2,1)S(1)} all-reduce(bf16[8,1024]{1,0:T(8,128)(2,1)S(1)} %convolution_convert_fusion.1), channel_id=1, replica_groups=mesh['ep'=8,'tp'=4] {'tp'}, use_global_device_ids=true, to_apply=%region_6.7 | all-reduce | flops 8192 | bytes 32768 | tf_op jit(solution)/shard_map/psum | solution.py:87
  34.2 0.6 fusion.34
  34.8 6.0 %all-to-all-start = ((bf16[8,8,128]{2,0,1:T(8,128)(2,1)}), bf16[8,8,128]{2,0,1:T(8,128)(2,1)S(1)}, u32[]{:S(2)}, u32[]{:S(2)}) async-start(bf16[8,8,128]{2,0,1:T(8,128)(2,1)} %fusion.34), calls=%async_computation | async-start | bytes 32768 | tf_op jit(solution)/shard_map/all_to_all | solution.py:91
  41.8 5.6 %all-to-all-done = bf16[8,8,128]{2,0,1:T(8,128)(2,1)S(1)} async-done(((bf16[8,8,128]{2,0,1:T(8,128)(2,1)}), bf16[8,8,128]{2,0,1:T(8,128)(2,1)S(1)}, u32[]{:S(2)}, u32[]{:S(2)}) %all-to-all-start) | async-done | bytes 16416 | tf_op jit(solution)/shard_map/all_to_all | solution.py:91
  47.4 0.9 scatter_custom_fusion
  48.3 9.3 %all_to_all.43 = bf16[8,32,128]{2,1,0:T(8,128)(2,1)S(1)} all-to-all(bf16[8,32,128]{2,1,0:T(8,128)(2,1)S(1)} %bitcast.126), channel_id=1, replica_groups=mesh['ep'=8,'tp'=4] {'ep'}, dimensions={0} | all-to-all | bytes 131072 | tf_op jit(solution)/shard_map/all_to_all | solution.py:101
  57.7 0.6 copy-done.7
  58.6 0.6 copy-done.6
  59.3 0.9 fusion
  60.3 1.2 %multiply_add_fusion = f32[8,1,128,256]{3,2,1,0:T(8,128)} fusion(f32[8,1,128,256]{3,2,1,0:T(8,128)S(1)} %copy-done.1, f32[8,256]{1,0:T(8,128)S(1)} %convert_element_type.117, f32[8,128]{1,0:T(8,128)S(1)} %get-tuple-element.30, f32[8]{0:T(128)S(1)} %get-tuple-element.24), kind=kLoop, calls=%fused_computation.18 | loop fusion | flops 786432 | bytes 2109472 | tf_op jit(solution)/shard_map/add | solution.py:78
  61.5 27.0 %all-reduce.2.cloned.1.call-done = bf16[1,32,1024]{2,1,0:T(8,128)(2,1)} async-done(((bf16[1,32,1024]{2,1,0:T(8,128)(2,1)}), bf16[1,32,1024]{2,1,0:T(8,128)(2,1)}) %all-reduce.2.cloned.1.call-update) | async-done | bytes 65552 | tf_op jit(solution)/shard_map/psum | solution.py:109
  88.5 1.1 copy.50
  90.1 2.3 %reduce.3 = bf16[1024,32]{1,0:T(8,128)(2,1)S(1)} reduce(bf16[1024,1,32]{2,1,0:T(2,128)(2,1)S(1)} %bitcast.121, bf16[]{:T(256)} %broadcast.215), dimensions={1}, to_apply=%bitcast.105.reduce_sub_computation | reduce | bytes 131074
  92.4 0.9 reshape.303
  93.3 5.5 %all-to-all-start.2 = ((bf16[8,2,2048]{2,1,0:T(2,128)(2,1)}), bf16[8,2,2048]{2,1,0:T(2,128)(2,1)S(1)}, u32[]{:S(2)}, u32[]{:S(2)}) async-start(bf16[8,2,2048]{2,1,0:T(2,128)(2,1)} %reshape.303), calls=%async_computation.2 | async-start | bytes 131072 | tf_op jit(solution)/shard_map/all_to_all | solution.py:110
  99.0 6.8 %all-to-all-done.2 = bf16[8,2,2048]{2,1,0:T(2,128)(2,1)S(1)} async-done(((bf16[8,2,2048]{2,1,0:T(2,128)(2,1)}), bf16[8,2,2048]{2,1,0:T(2,128)(2,1)S(1)}, u32[]{:S(2)}, u32[]{:S(2)}) %all-to-all-start.2) | async-done | bytes 65568 | tf_op jit(solution)/shard_map/all_to_all | solution.py:110
  106.4 0.7 gather_fusion
  107.3 0.6 add_convert_fusion
  (61 shorter events, 3.4 us)
Async XLA Ops:
  7.2 13.5 %copy-start = (bf16[256,1024]{1,0:T(8,128)(2,1)S(1)}, bf16[256,1024]{1,0:T(8,128)(2,1)}, u32[]{:S(2)}) copy-start(bf16[256,1024]{1,0:T(8,128)(2,1)} %param.30) | copy-start | bytes 1572868
  7.2 2.3 %copy-start.3 = (bf16[8,1024]{1,0:T(8,128)(2,1)S(1)}, bf16[8,1024]{1,0:T(8,128)(2,1)}, u32[]{:S(2)}) copy-start(bf16[8,1024]{1,0:T(8,128)(2,1)} %param.20) | copy-start | bytes 49156
  7.2 6.8 %copy-start.12 = (bf16[1024,128]{1,0:T(8,128)(2,1)S(1)}, bf16[1024,128]{1,0:T(8,128)(2,1)}, u32[]{:S(2)}) copy-start(bf16[1024,128]{1,0:T(8,128)(2,1)} %param.22) | copy-start | bytes 786436
  7.2 8.9 %copy-start.2 = (bf16[1024,256]{1,0:T(8,128)(2,1)S(1)}, bf16[1024,256]{1,0:T(8,128)(2,1)}, u32[]{:S(2)}) copy-start(bf16[1024,256]{1,0:T(8,128)(2,1)} %param.24) | copy-start | bytes 1572868
  7.2 12.6 %copy-start.1 = (f32[8,1,128,256]{3,2,1,0:T(8,128)S(1)}, f32[8,1,128,256]{3,2,1,0:T(8,128)}, u32[]{:S(2)}) copy-start(f32[8,1,128,256]{3,2,1,0:T(8,128)} %param.31) | copy-start | bytes 3145732
  14.0 5.8 %copy-start.11 = (f32[8,1]{0,1:T(1,128)}, f32[8,1]{0,1:T(1,128)S(1)}, u32[]{:S(2)}) copy-start(f32[8,1]{0,1:T(1,128)S(1)} %get-tuple-element.29) | copy-start | bytes 100
  18.3 0.7 copy-start.10
  20.6 0.7 copy-start.13
  34.8 6.0 %copy-start.8 = (s32[64,2]{0,1:T(2,128)S(1)}, s32[64,2]{0,1:T(2,128)}, u32[]{:S(2)}) copy-start(s32[64,2]{0,1:T(2,128)} %param.35) | copy-start | bytes 1540
  34.8 12.5 %all-to-all-start = ((bf16[8,8,128]{2,0,1:T(8,128)(2,1)}), bf16[8,8,128]{2,0,1:T(8,128)(2,1)S(1)}, u32[]{:S(2)}, u32[]{:S(2)}) async-start(bf16[8,8,128]{2,0,1:T(8,128)(2,1)} %fusion.34), calls=%async_computation | async-start | bytes 32768 | tf_op jit(solution)/shard_map/all_to_all | solution.py:91
  40.8 47.7 %all-reduce.2.cloned.1.call-start = ((), (), s32[]{:S(2)}) async-start(), calls=%async_computation.3 | async-start | bytes 131072 | tf_op jit(solution)/shard_map/psum | solution.py:109
  47.4 11.0 %copy-start.4 = (bf16[1,1024,128]{2,1,0:T(8,128)(2,1)S(1)}, bf16[1,1024,128]{2,1,0:T(8,128)(2,1)}, u32[]{:S(2)}) copy-start(bf16[1,1024,128]{2,1,0:T(8,128)(2,1)} %param.37) | copy-start | bytes 786436
  57.6 0.7 copy-start.7
  58.3 0.9 copy-start.6
  58.4 1.0 copy-start.5
  60.3 1.2 %copy-start.9 = (f32[64,2]{0,1:T(2,128)S(1)}, f32[64,2]{0,1:T(2,128)}, u32[]{:S(2)}) copy-start(f32[64,2]{0,1:T(2,128)} %param.36) | copy-start | bytes 1540
  93.3 12.4 %all-to-all-start.2 = ((bf16[8,2,2048]{2,1,0:T(2,128)(2,1)}), bf16[8,2,2048]{2,1,0:T(2,128)(2,1)S(1)}, u32[]{:S(2)}, u32[]{:S(2)}) async-start(bf16[8,2,2048]{2,1,0:T(2,128)(2,1)} %reshape.303), calls=%async_computation.2 | async-start | bytes 131072 | tf_op jit(solution)/shard_map/all_to_all | solution.py:110
Sparse Core Ops, SparseCore 0:
  60.4 28.0 all-reduce.1
where the time goes:
time: 116 us; the launch traced here: 115 us
  waiting for transfers between devices  39.4 us (34%)
  blocking collectives  22 us (19%)
  between operations  14.3 us (12%)
  starting transfers between devices  11.5 us (10%)
  other arithmetic  11.4 us (10%)
  local copies, waits for them, and re-layouts  8.14 us (7%)
  matrix products  7.98 us (7%)
    psum x1, waiting for transfers between devices, shards(): results = lax.psum(partial_value.astype(jnp.bfloat16), 'tp')  27 us
    psum x1, blocking collectives, shards(): lax.psum(jnp.dot(gated, w_out, preferred_element_type=jnp.float32).astype...  12.7 us
    all_to_all x1, blocking collectives, shards(): rows = lax.all_to_all(buffer, 'ep', split_axis=0, concat_axis=2, tiled=True)  9.29 us
    all_to_all x1, waiting for transfers between devices, shards(): lax.all_to_all(results, 'ep', split_axis=2, concat_axis=0, tiled=True)  6.79 us
    all_to_all x1, starting transfers between devices, shards(): lax.all_to_all(middle_rows, 'ep', split_axis=1, concat_axis=0, tiled=True)  5.97 us
    all_to_all x1, waiting for transfers between devices, shards(): lax.all_to_all(middle_rows, 'ep', split_axis=1, concat_axis=0, tiled=True)  5.58 us
    all_to_all x1, starting transfers between devices, shards(): lax.all_to_all(results, 'ep', split_axis=2, concat_axis=0, tiled=True)  5.52 us
    unnamed x33, local copies, waits for them, and re-layouts  4.59 us
  transfers between devices with their start and end apart: 3, of which 3 were waited for; matrix products, arithmetic and copies ran while one was open for 2% of the time, Pallas kernels for 0%

commit v1 on v0

--- a/solution.py
+++ b/solution.py
@@ -1,6 +1,10 @@
+import functools
+
 import jax
 import jax.numpy as jnp
 from jax import lax
+from jax.experimental import pallas as pl
+from jax.experimental.pallas import tpu as pltpu
 from jax.sharding import PartitionSpec as P
 
 EXPERT_CAPACITY = 32
@@ -117,9 +121,397 @@
     return (mixed, state[:, None], norm_state[:, None], new_max[:, None])
 
 
+MESH = pl.DeviceIdType.MESH
+
+
+def dot(a, b):
+    return jnp.dot(a, b, preferred_element_type=jnp.float32)
+
+
+def layer_kernel(
+    n_ep,
+    n_tp,
+    cap,
+    tokens_ref,
+    mix_gain_ref,
+    w_query_hbm,
+    w_key_hbm,
+    w_value_hbm,
+    w_ogate_hbm,
+    w_igate_ref,
+    w_fgate_ref,
+    forget_bias_ref,
+    head_gain_ref,
+    w_out_hbm,
+    memory_hbm,
+    normalizer_ref,
+    running_max_ref,
+    ffn_gain_ref,
+    route_ref,
+    route_weight_ref,
+    w_gate_hbm,
+    w_up_hbm,
+    w_down_hbm,
+    mixed_ref,
+    new_memory_hbm,
+    new_normalizer_ref,
+    new_max_ref,
+    w_query,
+    w_key,
+    w_value,
+    w_ogate,
+    w_out,
+    memory,
+    w_gate,
+    w_up,
+    w_down,
+    state_buf,
+    numer_buf,
+    tp_rows,
+    ep_rows,
+    sent_slots,
+    ep_slots,
+    tp_mixed,
+    load_sem,
+    store_sem,
+    tp_send,
+    tp_recv,
+    ep_send,
+    ep_recv,
+    slot_send,
+    slot_recv,
+    mix_send,
+    mix_recv,
+):
+    f32, bf16 = jnp.float32, jnp.bfloat16
+    ep, tp = lax.axis_index("ep"), lax.axis_index("tp")
+    tp_peers = [lax.rem(tp + d, n_tp) for d in range(1, n_tp)]
+    ep_peers = [lax.rem(ep + d, n_ep) for d in range(1, n_ep)]
+
+    barrier = pltpu.get_barrier_semaphore()
+    for peer in tp_peers:
+        pl.semaphore_signal(barrier, inc=1, device_id={"tp": peer}, device_id_type=MESH)
+    for peer in ep_peers:
+        pl.semaphore_signal(barrier, inc=1, device_id={"ep": peer}, device_id_type=MESH)
+
+    loads = [
+        pltpu.make_async_copy(source, target, load_sem.at[i])
+        for i, (source, target) in enumerate(
+            [
+                (w_query_hbm, w_query),
+                (w_key_hbm, w_key),
+                (w_value_hbm, w_value),
+                (w_ogate_hbm, w_ogate),
+                (memory_hbm, memory),
+                (w_out_hbm, w_out),
+                (w_gate_hbm, w_gate),
+                (w_up_hbm, w_up),
+                (w_down_hbm, w_down),
+            ]
+        )
+    ]
+    for load in loads:
+        load.start()
+
+    def normalized(floats, gain):
+        scale = lax.rsqrt(jnp.mean(floats * floats, axis=-1, keepdims=True) + EPS)
+        return (floats * scale * gain).astype(bf16)
+
+    own = tokens_ref.shape[0]
+    tokens = tokens_ref[...].astype(f32)
+    normed = normalized(tokens, mix_gain_ref[...])
+    normed_floats = normed.astype(f32)
+
+    def gate_logit(weight_ref):
+        weight = weight_ref[...].astype(f32)
+        pick = lax.broadcasted_iota(jnp.int32, weight.shape, 0) == tp
+        row = jnp.sum(jnp.where(pick, weight, 0.0), axis=0, keepdims=True)
+        return jnp.sum(normed_floats * row, axis=1, keepdims=True)
+
+    log_in = gate_logit(w_igate_ref)
+    bias = forget_bias_ref[...]
+    bias = jnp.sum(
+        jnp.where(lax.broadcasted_iota(jnp.int32, bias.shape, 1) == tp, bias, 0.0),
+        axis=1,
+        keepdims=True,
+    )
+    forget_pre = gate_logit(w_fgate_ref) + bias
+    log_forget = jnp.minimum(forget_pre, 0.0) - jnp.log1p(jnp.exp(-jnp.abs(forget_pre)))
+    eye = lax.broadcasted_iota(jnp.int32, (own, own), 0) == lax.broadcasted_iota(
+        jnp.int32, (own, own), 1
+    )
+    old_max = jnp.sum(jnp.where(eye, running_max_ref[...], 0.0), axis=1, keepdims=True)
+    new_max = jnp.maximum(log_forget + old_max, log_in)
+    keep = jnp.exp(log_forget + old_max - new_max)
+    admit = jnp.exp(log_in - new_max)
+    new_max_ref[...] = jnp.sum(jnp.where(eye, new_max, 0.0), axis=0, keepdims=True)
+
+    loads[0].wait()
+    query = dot(normed, w_query[...]).astype(bf16).astype(f32)
+    loads[1].wait()
+    key = dot(normed, w_key[...]).astype(bf16).astype(f32)
+    scaled_key = key * w_key.shape[1] ** (-0.5)
+    admitted = admit * scaled_key
+    loads[2].wait()
+    value = dot(normed, w_value[...]).astype(bf16).astype(f32)
+    loads[3].wait()
+    ogate = dot(normed, w_ogate[...]).astype(bf16).astype(f32)
+
+    norm_state = keep * normalizer_ref[:, 0, :] + admitted
+    new_normalizer_ref[:, 0, :] = norm_state
+    denom = jnp.sum(query * norm_state, axis=1, keepdims=True)
+
+    query_columns = query.T
+    key_columns = admitted.T
+    loads[4].wait()
+    stores = []
+    for t in range(own):
+        state = (
+            keep[t : t + 1, :] * memory[t]
+            + key_columns[:, t : t + 1] * value[t : t + 1, :]
+        )
+        state_buf[t] = state
+        numer_buf[t : t + 1, :] = jnp.sum(
+            query_columns[:, t : t + 1] * state, axis=0, keepdims=True
+        )
+        store = pltpu.make_async_copy(state_buf.at[t], new_memory_hbm.at[t], store_sem.at[t])
+        store.start()
+        stores.append(store)
+    read = numer_buf[...] / jnp.maximum(jnp.abs(denom), jnp.exp(-new_max))
+    scale = lax.rsqrt(jnp.mean(read * read, axis=-1, keepdims=True) + EPS)
+    gated = (jax.nn.sigmoid(ogate) * read * scale * head_gain_ref[...]).astype(bf16)
+    loads[5].wait()
+    tp_rows[tp] = dot(gated, w_out[...]).astype(bf16)
+
+    pl.semaphore_wait(barrier, n_tp - 1 + n_ep - 1)
+
+    def exchange(axis, me, peers, source, target, send_sem, recv_sem):
+        sends, receipts = [], []
+        for peer in peers:
+            send = pltpu.make_async_remote_copy(
+                src_ref=source(peer),
+                dst_ref=target.at[me],
+                send_sem=send_sem.at[peer],
+                recv_sem=recv_sem.at[me],
+                device_id={axis: peer},
+                device_id_type=MESH,
+            )
+            send.start()
+            sends.append(send)
+            receipts.append(
+                pltpu.make_async_remote_copy(
+                    src_ref=source(peer),
+                    dst_ref=target.at[peer],
+                    send_sem=send_sem.at[peer],
+                    recv_sem=recv_sem.at[peer],
+                    device_id={axis: peer},
+                    device_id_type=MESH,
+                )
+            )
+        return sends, receipts
+
+    sends, receipts = exchange(
+        "tp", tp, tp_peers, lambda peer: tp_rows.at[tp], tp_rows, tp_send, tp_recv
+    )
+    all_sends = sends
+
+    count = route_ref.shape[1]
+    topk = route_ref.shape[0]
+    experts = n_ep
+    earlier = (
+        lax.broadcasted_iota(jnp.int32, (count, count), 0)
+        < lax.broadcasted_iota(jnp.int32, (count, count), 1)
+    ).astype(bf16)
+    weight_rows = route_weight_ref[...]
+    weight_rows = weight_rows / jnp.sum(weight_rows, axis=0, keepdims=True)
+
+    def slot_rows(rows, expert):
+        named = route_ref[0:1, :] == expert
+        for j in range(1, topk):
+            named = named | (route_ref[j : j + 1, :] == expert)
+        named = named.astype(f32)
+        before = dot(named.astype(bf16), earlier)
+        slot = lax.broadcasted_iota(jnp.int32, (rows, count), 0) % cap
+        return jnp.where(before == slot.astype(f32), named, 0.0)
+
+    mine = slot_rows(cap, jnp.full((cap, count), ep, jnp.int32))
+    chosen_weight = jnp.zeros((1, count), f32)
+    for j in range(topk):
+        chosen_weight = chosen_weight + jnp.where(
+            route_ref[j : j + 1, :] == ep, weight_rows[j : j + 1, :], 0.0
+        )
+    slot_weight = jnp.sum(mine * chosen_weight, axis=1, keepdims=True)
+    mine = mine.astype(bf16)
+    every = experts * cap
+    combine = slot_rows(
+        every, lax.broadcasted_iota(jnp.int32, (every, count), 0) // cap
+    ).T.astype(bf16)
+
+    for receipt in receipts:
+        receipt.wait_recv()
+    summed = tp_rows[0].astype(f32)
+    for i in range(1, n_tp):
+        summed = summed + tp_rows[i].astype(f32)
+    ep_rows[ep] = (tokens + summed).astype(bf16)
+    sends, receipts = exchange(
+        "ep", ep, ep_peers, lambda peer: ep_rows.at[ep], ep_rows, ep_send, ep_recv
+    )
+    all_sends = all_sends + sends
+    for load in loads[6:]:
+        load.wait()
+    for receipt in receipts:
+        receipt.wait_recv()
+
+    width = tokens.shape[1]
+    middle = ep_rows[...].astype(f32).reshape(count, width).astype(bf16)
+    rows = normalized(dot(mine, middle), ffn_gain_ref[...])
+    gate_v = dot(rows, w_gate[...])
+    up_v = dot(rows, w_up[...])
+    activation = (gate_v * jax.nn.sigmoid(gate_v) * up_v).astype(bf16)
+    partial = (dot(activation, w_down[...]) * slot_weight).astype(bf16)
+    columns = width // n_ep
+    for c in range(n_ep):
+        sent_slots[c] = partial[:, c * columns : (c + 1) * columns]
+    sends, receipts = exchange(
+        "ep", ep, ep_peers, lambda peer: sent_slots.at[peer], ep_slots, slot_send, slot_recv
+    )
+    all_sends = all_sends + sends
+    ep_slots[ep] = sent_slots[ep]
+    own_columns = pl.ds(pl.multiple_of(ep * columns, columns), columns)
+    result = ep_rows[:, :, own_columns].astype(f32).reshape(count, columns)
+    for receipt in receipts:
+        receipt.wait_recv()
+    tp_mixed[tp] = dot(combine, ep_slots[...].reshape(every, columns)).astype(bf16)
+    sends, receipts = exchange(
+        "tp", tp, tp_peers, lambda peer: tp_mixed.at[tp], tp_mixed, mix_send, mix_recv
+    )
+    all_sends = all_sends + sends
+    for store in stores:
+        store.wait()
+    for receipt in receipts:
+        receipt.wait_recv()
+    added = tp_mixed[0].astype(f32)
+    for i in range(1, n_tp):
+        added = added + tp_mixed[i].astype(f32)
+    mixed_ref[...] = (result + added).astype(bf16)
+    for send in all_sends:
+        send.wait_send()
+
+
+def layer(
+    tokens,
+    mix_gain,
+    w_query,
+    w_key,
+    w_value,
+    w_ogate,
+    w_igate,
+    w_fgate,
+    forget_bias,
+    head_gain,
+    w_out,
+    memory,
+    normalizer,
+    running_max,
+    ffn_gain,
+    route,
+    route_weight,
+    w_gate,
+    w_up,
+    w_down,
+):
+    n_ep, n_tp = lax.axis_size("ep"), lax.axis_size("tp")
+    own, width = tokens.shape
+    columns = width // n_ep
+    if columns % 128 or own % 8 or w_gate.shape[0] != 1:
+        return shards(
+            tokens,
+            mix_gain,
+            w_query,
+            w_key,
+            w_value,
+            w_ogate,
+            w_igate,
+            w_fgate,
+            forget_bias,
+            head_gain,
+            w_out,
+            memory,
+            normalizer,
+            running_max,
+            ffn_gain,
+            route,
+            route_weight,
+            w_gate,
+            w_up,
+            w_down,
+        )
+    cap = EXPERT_CAPACITY
+    count = route.shape[0]
+    vmem = pl.BlockSpec(memory_space=pltpu.VMEM)
+    hbm = pl.BlockSpec(memory_space=pl.ANY)
+    bf16, f32 = jnp.bfloat16, jnp.float32
+    weights = [w_query, w_key, w_value, w_ogate, w_out, memory[:, 0], w_gate[0], w_up[0], w_down[0]]
+    dma = pltpu.SemaphoreType.DMA
+    mixed, new_memory, new_normalizer, new_max = pl.pallas_call(
+        functools.partial(layer_kernel, n_ep, n_tp, cap),
+        out_shape=(
+            jax.ShapeDtypeStruct((count, columns), bf16),
+            jax.ShapeDtypeStruct(memory[:, 0].shape, f32),
+            jax.ShapeDtypeStruct(normalizer.shape, f32),
+            jax.ShapeDtypeStruct((1, own), f32),
+        ),
+        in_specs=[vmem] * 2 + [hbm] * 4 + [vmem] * 4 + [hbm] * 2 + [vmem] * 5 + [hbm] * 3,
+        out_specs=(vmem, hbm, vmem, vmem),
+        scratch_shapes=[pltpu.VMEM(w.shape, w.dtype) for w in weights]
+        + [
+            pltpu.VMEM(memory[:, 0].shape, f32),
+            pltpu.VMEM((own, w_value.shape[1]), f32),
+            pltpu.VMEM((n_tp, own, width), bf16),
+            pltpu.VMEM((n_ep, own, width), bf16),
+            pltpu.VMEM((n_ep, cap, columns), bf16),
+            pltpu.VMEM((n_ep, cap, columns), bf16),
+            pltpu.VMEM((n_tp, count, columns), bf16),
+            dma((len(weights),)),
+            dma((own,)),
+            dma((n_tp,)),
+            dma((n_tp,)),
+            dma((n_ep,)),
+            dma((n_ep,)),
+            dma((n_ep,)),
+            dma((n_ep,)),
+            dma((n_tp,)),
+            dma((n_tp,)),
+        ],
+        compiler_params=pltpu.CompilerParams(collective_id=0, has_side_effects=True),
+    )(
+        tokens,
+        mix_gain[None],
+        w_query,
+        w_key,
+        w_value,
+        w_ogate,
+        w_igate.T,
+        w_fgate.T,
+        forget_bias[None],
+        head_gain[None],
+        w_out,
+        memory[:, 0],
+        normalizer,
+        running_max.T,
+        ffn_gain[None],
+        route.T,
+        route_weight.T,
+        w_gate[0],
+        w_up[0],
+        w_down[0],
+    )
+    return mixed, new_memory[:, None], new_normalizer, new_max.T
+
+
 def solution(mesh):
     return jax.shard_map(
-        shards,
+        layer,
         mesh=mesh,
         in_specs=(
             P("ep", None),

time: 116 us -> 29.4 us (0.25)
  waiting for transfers between devices: 39.4 us -> 0 us
  Pallas kernels: 0 us -> 23.8 us
  blocking collectives: 22 us -> 0 us
  between operations: 14.3 us -> 0.65 us
  starting transfers between devices: 11.5 us -> 0 us
  other arithmetic: 11.4 us -> 0 us
  matrix products: 7.98 us -> 0 us
  local copies, waits for them, and re-layouts: 8.14 us -> 4.77 us
    psum x1 -> x0, waiting for transfers between devices: 27 us -> none  [shards(): results = lax.psum(partial_value.astype(jnp.bfloat16), 'tp')]
    pallas_call x0 -> x1, Pallas kernels: none -> 23.8 us  [layer(): pl.pallas_call(functools.partial(layer_kernel, n_ep, n_tp, cap), out_shap...]
    psum x1 -> x0, blocking collectives: 12.7 us -> none  [shards(): lax.psum(jnp.dot(gated, w_out, preferred_element_type=jnp.float32).astype...]
    all_to_all x2 -> x0, waiting for transfers between devices: 12.4 us -> none  [the longest x1 6.79 us: shards(): lax.all_to_all(results, 'ep', split_axis=2, concat_axis=0, tiled=True)]
    all_to_all x2 -> x0, starting transfers between devices: 11.5 us -> none  [the longest x1 5.97 us: shards(): lax.all_to_all(middle_rows, 'ep', split_axis=1, concat_axis=0, tiled=True)]
    all_to_all x1 -> x0, blocking collectives: 9.29 us -> none  [shards(): rows = lax.all_to_all(buffer, 'ep', split_axis=0, concat_axis=2, tiled=True)]
    dot_general x10 -> x0, matrix products: 7.98 us -> none  [the longest x1 1.28 us: shards(): jnp.dot(normed, w_ogate, preferred_element_type=jnp.float32)]
    reduce_sum x8 -> x0, other arithmetic: 3.67 us -> none  [the longest x1 1.41 us: shards(): jnp.sum(forget_bias * head_pick)]
  transfers between devices with their start and end apart: 3 -> 0, of which waited for: 3 -> 0; matrix products, arithmetic and copies ran while one was open for 2% -> 0% of each run, Pallas kernels for 0% -> 0%
where the time goes in v1:
time: 29.4 us; the launch traced here: 29.2 us
  Pallas kernels  23.8 us (81%)
  local copies, waits for them, and re-layouts  4.77 us (16%)
  between operations  0.65 us (2%)
    pallas_call x1, Pallas kernels, layer(): pl.pallas_call(functools.partial(layer_kernel, n_ep, n_tp, cap), out_shap...  23.8 us
    unnamed x8, local copies, waits for them, and re-layouts  4.77 us

profile of v1, /device:TPU:0, one launch (start us, length us, event | category | flops | bytes accessed | tf_op | source)
XLA Modules:
  0.0 29.2 jit_solution(10813828071251067613)
XLA Ops:
  0.6 23.8 %shard_map.219 = (bf16[64,128]{1,0:T(8,128)(2,1)}, f32[8,128,256]{2,1,0:T(8,128)}, f32[8,1,128]{2,1,0:T(1,128)}, f32[1,8]{1,0:T(1,128)}) custom-call(bf16[8,1024]{1,0:T(8,128)(2,1)} %tokens_ref.1, f32[1,1024]{1,0:T(1,128)} %bitcast.24, bf16[1024,128]{1,0:T(8,128)(2,1)} %w_query_hbm.1, bf16[1024,128]{1,0:T(8,128)(2,1)} %w_key_hbm.1, ...), custom_call_target="tpu_custom_call" | custom-call | tf_op jit(solution)/shard_map/pallas_call | solution.py:456
  24.4 1.3 %copy.29 = bf16[64,128]{1,0:T(8,128)(2,1)} copy(bf16[64,128]{1,0:T(8,128)(2,1)} %get-tuple-element.20) | data formatting | bytes 32768
  25.7 0.0 copy-start
  25.7 2.3 %copy.30 = f32[8,1,128,256]{3,2,1,0:T(8,128)} copy(f32[8,1,128,256]{3,2,1,0:T(8,128)} %bitcast.17) | data formatting | bytes 2097152
  28.0 0.0 copy-done
  28.0 0.0 copy-start.1
  28.0 0.6 %copy.31 = f32[8,1,128]{2,1,0:T(1,128)} copy(f32[8,1,128]{2,1,0:T(1,128)S(1)} %copy-done) | data formatting | bytes 8192
  28.6 0.1 copy-done.1
  28.7 0.5 %copy.32 = f32[8,1]{0,1:T(1,128)} copy(f32[8,1]{0,1:T(1,128)S(1)} %bitcast.31) | data formatting | bytes 64
Async XLA Ops:
  25.7 2.3 %copy-start = (f32[8,1,128]{2,1,0:T(1,128)S(1)}, f32[8,1,128]{2,1,0:T(1,128)}, u32[]{:S(2)}) copy-start(f32[8,1,128]{2,1,0:T(1,128)} %get-tuple-element.22) | copy-start | bytes 12292
  28.0 0.7 %copy-start.1 = (f32[1,8]{1,0:T(1,128)S(1)}, f32[1,8]{1,0:T(1,128)}, u32[]{:S(2)}) copy-start(f32[1,8]{1,0:T(1,128)} %get-tuple-element.11) | copy-start | bytes 100

commit v2 on v1

--- a/solution.py
+++ b/solution.py
@@ -128,61 +128,73 @@
     return jnp.dot(a, b, preferred_element_type=jnp.float32)
 
 
-def layer_kernel(
-    n_ep,
-    n_tp,
-    cap,
-    tokens_ref,
-    mix_gain_ref,
-    w_query_hbm,
-    w_key_hbm,
-    w_value_hbm,
-    w_ogate_hbm,
-    w_igate_ref,
-    w_fgate_ref,
-    forget_bias_ref,
-    head_gain_ref,
-    w_out_hbm,
-    memory_hbm,
-    normalizer_ref,
-    running_max_ref,
-    ffn_gain_ref,
-    route_ref,
-    route_weight_ref,
-    w_gate_hbm,
-    w_up_hbm,
-    w_down_hbm,
-    mixed_ref,
-    new_memory_hbm,
-    new_normalizer_ref,
-    new_max_ref,
-    w_query,
-    w_key,
-    w_value,
-    w_ogate,
-    w_out,
-    memory,
-    w_gate,
-    w_up,
-    w_down,
-    state_buf,
-    numer_buf,
-    tp_rows,
-    ep_rows,
-    sent_slots,
-    ep_slots,
-    tp_mixed,
-    load_sem,
-    store_sem,
-    tp_send,
-    tp_recv,
-    ep_send,
-    ep_recv,
-    slot_send,
-    slot_recv,
-    mix_send,
-    mix_recv,
-):
+LOAD_ORDER = (
+    0,
+    1,
+    6,
+    7,
+    8,
+    13,
+    2,
+    3,
+    4,
+    5,
+    12,
+    11,
+    9,
+    10,
+    15,
+    16,
+    14,
+    17,
+    18,
+    19,
+)
+
+
+def layer_kernel(n_ep, n_tp, cap, *refs):
+    arguments, refs = refs[: len(LOAD_ORDER)], refs[len(LOAD_ORDER) :]
+    (mixed_ref, state_buf, new_normalizer_ref, new_max_ref), refs = refs[:4], refs[4:]
+    staged, refs = refs[: len(LOAD_ORDER)], refs[len(LOAD_ORDER) :]
+    (
+        tokens_ref,
+        mix_gain_ref,
+        w_query,
+        w_key,
+        w_value,
+        w_ogate,
+        w_igate_ref,
+        w_fgate_ref,
+        forget_bias_ref,
+        head_gain_ref,
+        w_out,
+        memory,
+        normalizer_ref,
+        running_max_ref,
+        ffn_gain_ref,
+        route_ref,
+        route_weight_ref,
+        w_gate,
+        w_up,
+        w_down,
+    ) = staged
+    (
+        numer_buf,
+        tp_rows,
+        ep_rows,
+        sent_slots,
+        ep_slots,
+        tp_mixed,
+        load_sem,
+        tp_send,
+        tp_recv,
+        ep_send,
+        ep_recv,
+        slot_send,
+        slot_recv,
+        mix_send,
+        mix_recv,
+    ) = refs
     f32, bf16 = jnp.float32, jnp.bfloat16
     ep, tp = lax.axis_index("ep"), lax.axis_index("tp")
     tp_peers = [lax.rem(tp + d, n_tp) for d in range(1, n_tp)]
@@ -194,30 +206,23 @@
     for peer in ep_peers:
         pl.semaphore_signal(barrier, inc=1, device_id={"ep": peer}, device_id_type=MESH)
 
-    loads = [
-        pltpu.make_async_copy(source, target, load_sem.at[i])
-        for i, (source, target) in enumerate(
-            [
-                (w_query_hbm, w_query),
-                (w_key_hbm, w_key),
-                (w_value_hbm, w_value),
-                (w_ogate_hbm, w_ogate),
-                (memory_hbm, memory),
-                (w_out_hbm, w_out),
-                (w_gate_hbm, w_gate),
-                (w_up_hbm, w_up),
-                (w_down_hbm, w_down),
-            ]
-        )
-    ]
-    for load in loads:
-        load.start()
+    loads = {}
+    for i in LOAD_ORDER:
+        loads[i] = pltpu.make_async_copy(arguments[i], staged[i], load_sem.at[i])
+        loads[i].start()
+
+    def arrived(*which):
+        for ref in which:
+            for i, target in enumerate(staged):
+                if target is ref:
+                    loads[i].wait()
 
     def normalized(floats, gain):
         scale = lax.rsqrt(jnp.mean(floats * floats, axis=-1, keepdims=True) + EPS)
         return (floats * scale * gain).astype(bf16)
 
     own = tokens_ref.shape[0]
+    arrived(tokens_ref, mix_gain_ref)
     tokens = tokens_ref[...].astype(f32)
     normed = normalized(tokens, mix_gain_ref[...])
     normed_floats = normed.astype(f32)
@@ -228,6 +233,7 @@
         row = jnp.sum(jnp.where(pick, weight, 0.0), axis=0, keepdims=True)
         return jnp.sum(normed_floats * row, axis=1, keepdims=True)
 
+    arrived(w_igate_ref, w_fgate_ref, forget_bias_ref, running_max_ref)
     log_in = gate_logit(w_igate_ref)
     bias = forget_bias_ref[...]
     bias = jnp.sum(
@@ -246,15 +252,15 @@
     admit = jnp.exp(log_in - new_max)
     new_max_ref[...] = jnp.sum(jnp.where(eye, new_max, 0.0), axis=0, keepdims=True)
 
-    loads[0].wait()
+    arrived(w_query)
     query = dot(normed, w_query[...]).astype(bf16).astype(f32)
-    loads[1].wait()
+    arrived(w_key)
     key = dot(normed, w_key[...]).astype(bf16).astype(f32)
     scaled_key = key * w_key.shape[1] ** (-0.5)
     admitted = admit * scaled_key
-    loads[2].wait()
+    arrived(w_value)
     value = dot(normed, w_value[...]).astype(bf16).astype(f32)
-    loads[3].wait()
+    arrived(w_ogate, normalizer_ref)
     ogate = dot(normed, w_ogate[...]).astype(bf16).astype(f32)
 
     norm_state = keep * normalizer_ref[:, 0, :] + admitted
@@ -263,8 +269,7 @@
 
     query_columns = query.T
     key_columns = admitted.T
-    loads[4].wait()
-    stores = []
+    arrived(memory)
     for t in range(own):
         state = (
             keep[t : t + 1, :] * memory[t]
@@ -274,13 +279,11 @@
         numer_buf[t : t + 1, :] = jnp.sum(
             query_columns[:, t : t + 1] * state, axis=0, keepdims=True
         )
-        store = pltpu.make_async_copy(state_buf.at[t], new_memory_hbm.at[t], store_sem.at[t])
-        store.start()
-        stores.append(store)
+    arrived(head_gain_ref)
     read = numer_buf[...] / jnp.maximum(jnp.abs(denom), jnp.exp(-new_max))
     scale = lax.rsqrt(jnp.mean(read * read, axis=-1, keepdims=True) + EPS)
     gated = (jax.nn.sigmoid(ogate) * read * scale * head_gain_ref[...]).astype(bf16)
-    loads[5].wait()
+    arrived(w_out)
     tp_rows[tp] = dot(gated, w_out[...]).astype(bf16)
 
     pl.semaphore_wait(barrier, n_tp - 1 + n_ep - 1)
@@ -315,6 +318,7 @@
     )
     all_sends = sends
 
+    arrived(route_ref, route_weight_ref)
     count = route_ref.shape[1]
     topk = route_ref.shape[0]
     experts = n_ep
@@ -357,8 +361,7 @@
         "ep", ep, ep_peers, lambda peer: ep_rows.at[ep], ep_rows, ep_send, ep_recv
     )
     all_sends = all_sends + sends
-    for load in loads[6:]:
-        load.wait()
+    arrived(ffn_gain_ref, w_gate, w_up, w_down)
     for receipt in receipts:
         receipt.wait_recv()
 
@@ -386,8 +389,6 @@
         "tp", tp, tp_peers, lambda peer: tp_mixed.at[tp], tp_mixed, mix_send, mix_recv
     )
     all_sends = all_sends + sends
-    for store in stores:
-        store.wait()
     for receipt in receipts:
         receipt.wait_recv()
     added = tp_mixed[0].astype(f32)
@@ -396,6 +397,19 @@
     mixed_ref[...] = (result + added).astype(bf16)
     for send in all_sends:
         send.wait_send()
+
+
+def write_results(*refs):
+    sem = refs[-1]
+    half = (len(refs) - 1) // 2
+    copies = [
+        pltpu.make_async_copy(source, target, sem.at[i])
+        for i, (source, target) in enumerate(zip(refs[:half], refs[half:-1]))
+    ]
+    for copy in copies:
+        copy.start()
+    for copy in copies:
+        copy.wait()
 
 
 def layer(
@@ -448,43 +462,10 @@
         )
     cap = EXPERT_CAPACITY
     count = route.shape[0]
+    anywhere = pl.BlockSpec(memory_space=pltpu.HBM)
     vmem = pl.BlockSpec(memory_space=pltpu.VMEM)
-    hbm = pl.BlockSpec(memory_space=pl.ANY)
     bf16, f32 = jnp.bfloat16, jnp.float32
-    weights = [w_query, w_key, w_value, w_ogate, w_out, memory[:, 0], w_gate[0], w_up[0], w_down[0]]
-    dma = pltpu.SemaphoreType.DMA
-    mixed, new_memory, new_normalizer, new_max = pl.pallas_call(
-        functools.partial(layer_kernel, n_ep, n_tp, cap),
-        out_shape=(
-            jax.ShapeDtypeStruct((count, columns), bf16),
-            jax.ShapeDtypeStruct(memory[:, 0].shape, f32),
-            jax.ShapeDtypeStruct(normalizer.shape, f32),
-            jax.ShapeDtypeStruct((1, own), f32),
-        ),
-        in_specs=[vmem] * 2 + [hbm] * 4 + [vmem] * 4 + [hbm] * 2 + [vmem] * 5 + [hbm] * 3,
-        out_specs=(vmem, hbm, vmem, vmem),
-        scratch_shapes=[pltpu.VMEM(w.shape, w.dtype) for w in weights]
-        + [
-            pltpu.VMEM(memory[:, 0].shape, f32),
-            pltpu.VMEM((own, w_value.shape[1]), f32),
-            pltpu.VMEM((n_tp, own, width), bf16),
-            pltpu.VMEM((n_ep, own, width), bf16),
-            pltpu.VMEM((n_ep, cap, columns), bf16),
-            pltpu.VMEM((n_ep, cap, columns), bf16),
-            pltpu.VMEM((n_tp, count, columns), bf16),
-            dma((len(weights),)),
-            dma((own,)),
-            dma((n_tp,)),
-            dma((n_tp,)),
-            dma((n_ep,)),
-            dma((n_ep,)),
-            dma((n_ep,)),
-            dma((n_ep,)),
-            dma((n_tp,)),
-            dma((n_tp,)),
-        ],
-        compiler_params=pltpu.CompilerParams(collective_id=0, has_side_effects=True),
-    )(
+    operands = [
         tokens,
         mix_gain[None],
         w_query,
@@ -505,7 +486,49 @@
         w_gate[0],
         w_up[0],
         w_down[0],
-    )
+    ]
+    dma = pltpu.SemaphoreType.DMA
+    results = [
+        ((count, columns), bf16),
+        (memory[:, 0].shape, f32),
+        (normalizer.shape, f32),
+        ((1, own), f32),
+    ]
+    held = pl.pallas_call(
+        functools.partial(layer_kernel, n_ep, n_tp, cap),
+        out_shape=tuple(pltpu.VMEM(*result) for result in results),
+        in_specs=[anywhere] * len(operands),
+        out_specs=(vmem,) * len(results),
+        scratch_shapes=[pltpu.VMEM(a.shape, a.dtype) for a in operands]
+        + [
+            pltpu.VMEM((own, w_value.shape[1]), f32),
+            pltpu.VMEM((n_tp, own, width), bf16),
+            pltpu.VMEM((n_ep, own, width), bf16),
+            pltpu.VMEM((n_ep, cap, columns), bf16),
+            pltpu.VMEM((n_ep, cap, columns), bf16),
+            pltpu.VMEM((n_tp, count, columns), bf16),
+            dma((len(operands),)),
+            dma((n_tp,)),
+            dma((n_tp,)),
+            dma((n_ep,)),
+            dma((n_ep,)),
+            dma((n_ep,)),
+            dma((n_ep,)),
+            dma((n_tp,)),
+            dma((n_tp,)),
+        ],
+        compiler_params=pltpu.CompilerParams(
+            collective_id=0, has_side_effects=True
+        ),
+    )(*operands)
+    mixed, new_memory, new_normalizer, new_max = pl.pallas_call(
+        write_results,
+        out_shape=tuple(jax.ShapeDtypeStruct(*result) for result in results),
+        in_specs=[vmem] * len(results),
+        out_specs=(anywhere,) * len(results),
+        scratch_shapes=[dma((len(results),))],
+        compiler_params=pltpu.CompilerParams(vmem_limit_bytes=1024 * 1024),
+    )(*held)
     return mixed, new_memory[:, None], new_normalizer, new_max.T
 
 

time: 29.4 us -> 24.3 us (0.83)
  local copies, waits for them, and re-layouts: 4.77 us -> 0 us
  Pallas kernels: 23.8 us -> 23.4 us
    unnamed x8 -> x0, local copies, waits for them, and re-layouts: 4.77 us -> none
    pallas_call x1, Pallas kernels: 23.8 us -> 22.4 us  [layer(): pl.pallas_call(functools.partial(layer_kernel, n_ep, n_tp, cap), out_shap...]
    pallas_call x0 -> x1, Pallas kernels: none -> 1.02 us  [layer(): pl.pallas_call(write_results, out_shape=tuple((jax.ShapeDtypeStruct(*resu...]
where the time goes in v2:
time: 24.3 us; the launch traced here: 24 us
  Pallas kernels  23.4 us (96%)
  between operations  0.65 us (3%)
    pallas_call x1, Pallas kernels, layer(): pl.pallas_call(functools.partial(layer_kernel, n_ep, n_tp, cap), out_shap...  22.4 us
    pallas_call x1, Pallas kernels, layer(): pl.pallas_call(write_results, out_shape=tuple((jax.ShapeDtypeStruct(*resu...  1.02 us

profile of v2, /device:TPU:0, one launch (start us, length us, event | category | flops | bytes accessed | tf_op | source)
XLA Modules:
  0.0 24.0 jit_solution(15849645282485053581)
XLA Ops:
  0.6 22.4 %shard_map.219 = (bf16[64,128]{1,0:T(8,128)(2,1)S(1)}, f32[8,128,256]{2,1,0:T(8,128)S(1)}, f32[8,1,128]{2,1,0:T(1,128)S(1)}, f32[1,8]{1,0:T(1,128)S(1)}) custom-call(bf16[8,1024]{1,0:T(8,128)(2,1)} %refs_0_.1, f32[1,1024]{1,0:T(1,128)} %bitcast.23, bf16[1024,128]{1,0:T(8,128)(2,1)} %refs_2_.1, bf16[1024,128]{1,0:T(8,128)(2,1)} %refs_3_.1, ...), custom_call_target="tpu_custom_call" | custom-call | tf_op jit(solution)/shard_map/pallas_call | solution.py:497
  23.0 1.0 %shard_map.220 = (bf16[64,128]{1,0:T(8,128)(2,1)}, f32[8,128,256]{2,1,0:T(8,128)}, f32[8,1,128]{2,1,0:T(1,128)}, f32[1,8]{1,0:T(1,128)}) custom-call(bf16[64,128]{1,0:T(8,128)(2,1)S(1)} %get-tuple-element.12.refs_0_, f32[8,128,256]{2,1,0:T(8,128)S(1)} %get-tuple-element.13.refs_1_, f32[8,1,128]{2,1,0:T(1,128)S(1)} %get-tuple-element.14.refs_2_, ...), custom_call_target="tpu_custom_call" | custom-call | tf_op jit(solution)/shard_map/pallas_call | solution.py:524

commit v3 on v2

--- a/solution.py
+++ b/solution.py
@@ -194,17 +194,46 @@
         slot_recv,
         mix_send,
         mix_recv,
+        round_sem,
     ) = refs
     f32, bf16 = jnp.float32, jnp.bfloat16
     ep, tp = lax.axis_index("ep"), lax.axis_index("tp")
-    tp_peers = [lax.rem(tp + d, n_tp) for d in range(1, n_tp)]
-    ep_peers = [lax.rem(ep + d, n_ep) for d in range(1, n_ep)]
+    tp_peers = [
+        lax.rem(tp + d, n_tp)
+        for d in sorted(range(1, n_tp), key=lambda d: -min(d, n_tp - d))
+    ]
+    ep_peers = []
+    for i in range(n_ep - 1):
+        low, high = i, n_ep - 1 - i
+        up = jnp.where(high > ep, high, high - 1)
+        down = jnp.where(low < ep, low, low + 1)
+        ep_peers.append(jnp.where(2 * ep < n_ep, up, down))
+
+    beside = ep + 1 - 2 * lax.rem(ep, 2)
+    near = 1 + (ep >= 2).astype(jnp.int32) + (ep < n_ep - 2).astype(jnp.int32)
+    rounds = n_ep // 2 - 1
+
+    def greet(sem):
+        pl.semaphore_signal(sem, inc=1, device_id={"ep": beside}, device_id_type=MESH)
+
+        @pl.when(ep >= 2)
+        def _():
+            pl.semaphore_signal(sem, inc=1, device_id={"ep": ep - 2}, device_id_type=MESH)
+
+        @pl.when(ep < n_ep - 2)
+        def _():
+            pl.semaphore_signal(sem, inc=1, device_id={"ep": ep + 2}, device_id_type=MESH)
+
+    def heard(i):
+        if i < rounds:
+            pl.semaphore_wait(round_sem.at[i], near)
+            if i + 1 < rounds:
+                greet(round_sem.at[i + 1])
 
     barrier = pltpu.get_barrier_semaphore()
     for peer in tp_peers:
         pl.semaphore_signal(barrier, inc=1, device_id={"tp": peer}, device_id_type=MESH)
-    for peer in ep_peers:
-        pl.semaphore_signal(barrier, inc=1, device_id={"ep": peer}, device_id_type=MESH)
+    greet(barrier)
 
     loads = {}
     for i in LOAD_ORDER:
@@ -266,6 +295,10 @@
     norm_state = keep * normalizer_ref[:, 0, :] + admitted
     new_normalizer_ref[:, 0, :] = norm_state
     denom = jnp.sum(query * norm_state, axis=1, keepdims=True)
+
+    pl.semaphore_wait(barrier, n_tp - 1 + near)
+    if rounds:
+        greet(round_sem.at[0])
 
     query_columns = query.T
     key_columns = admitted.T
@@ -285,8 +318,6 @@
     gated = (jax.nn.sigmoid(ogate) * read * scale * head_gain_ref[...]).astype(bf16)
     arrived(w_out)
     tp_rows[tp] = dot(gated, w_out[...]).astype(bf16)
-
-    pl.semaphore_wait(barrier, n_tp - 1 + n_ep - 1)
 
     def exchange(axis, me, peers, source, target, send_sem, recv_sem):
         sends, receipts = [], []
@@ -317,6 +348,7 @@
         "tp", tp, tp_peers, lambda peer: tp_rows.at[tp], tp_rows, tp_send, tp_recv
     )
     all_sends = sends
+    heard(0)
 
     arrived(route_ref, route_weight_ref)
     count = route_ref.shape[1]
@@ -350,12 +382,15 @@
     combine = slot_rows(
         every, lax.broadcasted_iota(jnp.int32, (every, count), 0) // cap
     ).T.astype(bf16)
+    heard(1)
 
     for receipt in receipts:
         receipt.wait_recv()
     summed = tp_rows[0].astype(f32)
     for i in range(1, n_tp):
         summed = summed + tp_rows[i].astype(f32)
+    for i in range(2, rounds):
+        heard(i)
     ep_rows[ep] = (tokens + summed).astype(bf16)
     sends, receipts = exchange(
         "ep", ep, ep_peers, lambda peer: ep_rows.at[ep], ep_rows, ep_send, ep_recv
@@ -437,7 +472,7 @@
     n_ep, n_tp = lax.axis_size("ep"), lax.axis_size("tp")
     own, width = tokens.shape
     columns = width // n_ep
-    if columns % 128 or own % 8 or w_gate.shape[0] != 1:
+    if columns % 128 or own % 8 or n_ep % 2 or w_gate.shape[0] != 1:
         return shards(
             tokens,
             mix_gain,
@@ -516,6 +551,7 @@
             dma((n_ep,)),
             dma((n_tp,)),
             dma((n_tp,)),
+            pltpu.SemaphoreType.REGULAR((max(1, n_ep // 2 - 1),)),
         ],
         compiler_params=pltpu.CompilerParams(
             collective_id=0, has_side_effects=True

time: 24.3 us -> 23.4 us (0.963)
  Pallas kernels: 23.4 us -> 22.5 us
    pallas_call x1, Pallas kernels: 22.4 us -> 21.5 us  [layer(): pl.pallas_call(functools.partial(layer_kernel, n_ep, n_tp, cap), out_shap...]
where the time goes in v3:
time: 23.4 us; the launch traced here: 23.2 us
  Pallas kernels  22.5 us (96%)
  between operations  0.65 us (3%)
    pallas_call x1, Pallas kernels, layer(): pl.pallas_call(functools.partial(layer_kernel, n_ep, n_tp, cap), out_shap...  21.5 us
    pallas_call x1, Pallas kernels, layer(): pl.pallas_call(write_results, out_shape=tuple((jax.ShapeDtypeStruct(*resu...  1.02 us

profile of v3, /device:TPU:0, one launch (start us, length us, event | category | flops | bytes accessed | tf_op | source)
XLA Modules:
  0.0 23.2 jit_solution(2572898966956080968)
XLA Ops:
  0.6 21.5 %shard_map.219 = (bf16[64,128]{1,0:T(8,128)(2,1)S(1)}, f32[8,128,256]{2,1,0:T(8,128)S(1)}, f32[8,1,128]{2,1,0:T(1,128)S(1)}, f32[1,8]{1,0:T(1,128)S(1)}) custom-call(bf16[8,1024]{1,0:T(8,128)(2,1)} %refs_0_.1, f32[1,1024]{1,0:T(1,128)} %bitcast.23, bf16[1024,128]{1,0:T(8,128)(2,1)} %refs_2_.1, bf16[1024,128]{1,0:T(8,128)(2,1)} %refs_3_.1, ...), custom_call_target="tpu_custom_call" | custom-call | tf_op jit(solution)/shard_map/pallas_call | solution.py:532
  22.2 1.0 %shard_map.220 = (bf16[64,128]{1,0:T(8,128)(2,1)}, f32[8,128,256]{2,1,0:T(8,128)}, f32[8,1,128]{2,1,0:T(1,128)}, f32[1,8]{1,0:T(1,128)}) custom-call(bf16[64,128]{1,0:T(8,128)(2,1)S(1)} %get-tuple-element.12.refs_0_, f32[8,128,256]{2,1,0:T(8,128)S(1)} %get-tuple-element.13.refs_1_, f32[8,1,128]{2,1,0:T(1,128)S(1)} %get-tuple-element.14.refs_2_, ...), custom_call_target="tpu_custom_call" | custom-call | tf_op jit(solution)/shard_map/pallas_call | solution.py:560

commit v4 on v2

--- a/solution.py
+++ b/solution.py
@@ -180,6 +180,7 @@
     ) = staged
     (
         numer_buf,
+        tp_out,
         tp_rows,
         ep_rows,
         sent_slots,
@@ -190,6 +191,8 @@
         tp_recv,
         ep_send,
         ep_recv,
+        pass_send,
+        pass_recv,
         slot_send,
         slot_recv,
         mix_send,
@@ -197,8 +200,16 @@
     ) = refs
     f32, bf16 = jnp.float32, jnp.bfloat16
     ep, tp = lax.axis_index("ep"), lax.axis_index("tp")
-    tp_peers = [lax.rem(tp + d, n_tp) for d in range(1, n_tp)]
-    ep_peers = [lax.rem(ep + d, n_ep) for d in range(1, n_ep)]
+    tp_peers = [
+        lax.rem(tp + d, n_tp)
+        for d in sorted(range(1, n_tp), key=lambda d: -min(d, n_tp - d))
+    ]
+    ep_peers = []
+    for i in range(n_ep - 1):
+        low, high = i, n_ep - 1 - i
+        up = jnp.where(high > ep, high, high - 1)
+        down = jnp.where(low < ep, low, low + 1)
+        ep_peers.append(jnp.where(2 * ep < n_ep, up, down))
 
     barrier = pltpu.get_barrier_semaphore()
     for peer in tp_peers:
@@ -284,7 +295,11 @@
     scale = lax.rsqrt(jnp.mean(read * read, axis=-1, keepdims=True) + EPS)
     gated = (jax.nn.sigmoid(ogate) * read * scale * head_gain_ref[...]).astype(bf16)
     arrived(w_out)
-    tp_rows[tp] = dot(gated, w_out[...]).astype(bf16)
+    partial = dot(gated, w_out[...]).astype(bf16)
+    half_width = partial.shape[1] // 2
+    core = lax.rem(tp, 2)
+    for h in range(2):
+        tp_out[h] = partial[:, h * half_width : (h + 1) * half_width]
 
     pl.semaphore_wait(barrier, n_tp - 1 + n_ep - 1)
 
@@ -293,7 +308,7 @@
         for peer in peers:
             send = pltpu.make_async_remote_copy(
                 src_ref=source(peer),
-                dst_ref=target.at[me],
+                dst_ref=target(me),
                 send_sem=send_sem.at[peer],
                 recv_sem=recv_sem.at[me],
                 device_id={axis: peer},
@@ -304,7 +319,7 @@
             receipts.append(
                 pltpu.make_async_remote_copy(
                     src_ref=source(peer),
-                    dst_ref=target.at[peer],
+                    dst_ref=target(peer),
                     send_sem=send_sem.at[peer],
                     recv_sem=recv_sem.at[peer],
                     device_id={axis: peer},
@@ -314,8 +329,15 @@
         return sends, receipts
 
     sends, receipts = exchange(
-        "tp", tp, tp_peers, lambda peer: tp_rows.at[tp], tp_rows, tp_send, tp_recv
-    )
+        "tp",
+        tp,
+        tp_peers,
+        lambda peer: tp_out.at[lax.rem(peer, 2)],
+        lambda i: tp_rows.at[i],
+        tp_send,
+        tp_recv,
+    )
+    tp_rows[tp] = tp_out[core]
     all_sends = sends
 
     arrived(route_ref, route_weight_ref)
@@ -356,18 +378,52 @@
     summed = tp_rows[0].astype(f32)
     for i in range(1, n_tp):
         summed = summed + tp_rows[i].astype(f32)
-    ep_rows[ep] = (tokens + summed).astype(bf16)
+    own_half = pl.ds(pl.multiple_of(core * half_width, half_width), half_width)
+    ep_rows[core, ep] = (tokens_ref[:, own_half].astype(f32) + summed).astype(bf16)
     sends, receipts = exchange(
-        "ep", ep, ep_peers, lambda peer: ep_rows.at[ep], ep_rows, ep_send, ep_recv
+        "ep",
+        ep,
+        ep_peers,
+        lambda peer: ep_rows.at[core, ep],
+        lambda i: ep_rows.at[core, i],
+        ep_send,
+        ep_recv,
     )
     all_sends = all_sends + sends
+
+    def pass_on(i):
+        send = pltpu.make_async_remote_copy(
+            src_ref=ep_rows.at[core, i],
+            dst_ref=ep_rows.at[core, i],
+            send_sem=pass_send.at[i],
+            recv_sem=pass_recv.at[i],
+            device_id={"tp": tp + 1 - 2 * core},
+            device_id_type=MESH,
+        )
+        send.start()
+        return send
+
+    all_sends = all_sends + [pass_on(ep)]
+    for peer, receipt in reversed(list(zip(ep_peers, receipts))):
+        receipt.wait_recv()
+        all_sends = all_sends + [pass_on(peer)]
     arrived(ffn_gain_ref, w_gate, w_up, w_down)
-    for receipt in receipts:
-        receipt.wait_recv()
-
-    width = tokens.shape[1]
-    middle = ep_rows[...].astype(f32).reshape(count, width).astype(bf16)
-    rows = normalized(dot(mine, middle), ffn_gain_ref[...])
+    for i in range(n_ep):
+        pltpu.make_async_remote_copy(
+            src_ref=ep_rows.at[1 - core, i],
+            dst_ref=ep_rows.at[1 - core, i],
+            send_sem=pass_send.at[i],
+            recv_sem=pass_recv.at[i],
+            device_id={"tp": tp + 1 - 2 * core},
+            device_id_type=MESH,
+        ).wait_recv()
+
+    halves = [
+        dot(mine, ep_rows[h].astype(f32).reshape(count, half_width).astype(bf16))
+        for h in range(2)
+    ]
+    width = 2 * half_width
+    rows = normalized(jnp.concatenate(halves, axis=1), ffn_gain_ref[...])
     gate_v = dot(rows, w_gate[...])
     up_v = dot(rows, w_up[...])
     activation = (gate_v * jax.nn.sigmoid(gate_v) * up_v).astype(bf16)
@@ -375,26 +431,60 @@
     columns = width // n_ep
     for c in range(n_ep):
         sent_slots[c] = partial[:, c * columns : (c + 1) * columns]
-    sends, receipts = exchange(
-        "ep", ep, ep_peers, lambda peer: sent_slots.at[peer], ep_slots, slot_send, slot_recv
-    )
-    all_sends = all_sends + sends
-    ep_slots[ep] = sent_slots[ep]
-    own_columns = pl.ds(pl.multiple_of(ep * columns, columns), columns)
-    result = ep_rows[:, :, own_columns].astype(f32).reshape(count, columns)
+    pairs = n_tp // 2
+    pair = tp // 2
+    receipts = []
+
+    def expert_copy(source, target, to, chip, sem_of, i):
+        return pltpu.make_async_remote_copy(
+            src_ref=source,
+            dst_ref=target,
+            send_sem=slot_send.at[chip, to],
+            recv_sem=slot_recv.at[sem_of, i],
+            device_id={"ep": to, "tp": 2 * chip + core},
+            device_id_type=MESH,
+        )
+
+    for peer in ep_peers + [ep]:
+        for d in reversed(range(pairs)):
+            if d or peer is not ep:
+                chip = lax.rem(pair + d, pairs)
+                send = expert_copy(
+                    sent_slots.at[peer], ep_slots.at[pair, ep], peer, chip, pair, ep
+                )
+                send.start()
+                all_sends = all_sends + [send]
+                receipts.append(
+                    expert_copy(
+                        sent_slots.at[peer], ep_slots.at[chip, peer], peer, chip, chip, peer
+                    )
+                )
+    ep_slots[pair, ep] = sent_slots[ep]
+    per_half = n_ep // 2
+    offset = pl.multiple_of(lax.rem(ep, per_half) * columns, columns)
+    result = ep_rows[ep // per_half, :, :, pl.ds(offset, columns)].astype(f32).reshape(count, columns)
     for receipt in receipts:
         receipt.wait_recv()
-    tp_mixed[tp] = dot(combine, ep_slots[...].reshape(every, columns)).astype(bf16)
-    sends, receipts = exchange(
-        "tp", tp, tp_peers, lambda peer: tp_mixed.at[tp], tp_mixed, mix_send, mix_recv
-    )
-    all_sends = all_sends + sends
-    for receipt in receipts:
-        receipt.wait_recv()
-    added = tp_mixed[0].astype(f32)
-    for i in range(1, n_tp):
-        added = added + tp_mixed[i].astype(f32)
+    gathered = dot(combine, ep_slots[0].reshape(every, columns))
+    for i in range(1, pairs):
+        gathered = gathered + dot(combine, ep_slots[i].reshape(every, columns))
+    tp_mixed[core] = gathered.astype(bf16)
+    last = [
+        pltpu.make_async_remote_copy(
+            src_ref=tp_mixed.at[i],
+            dst_ref=tp_mixed.at[i],
+            send_sem=mix_send.at[i],
+            recv_sem=mix_recv.at[i],
+            device_id={"tp": tp + 1 - 2 * core},
+            device_id_type=MESH,
+        )
+        for i in (core, 1 - core)
+    ]
+    last[0].start()
+    last[1].wait_recv()
+    added = tp_mixed[0].astype(f32) + tp_mixed[1].astype(f32)
     mixed_ref[...] = (result + added).astype(bf16)
+    last[0].wait_send()
     for send in all_sends:
         send.wait_send()
 
@@ -437,7 +527,7 @@
     n_ep, n_tp = lax.axis_size("ep"), lax.axis_size("tp")
     own, width = tokens.shape
     columns = width // n_ep
-    if columns % 128 or own % 8 or w_gate.shape[0] != 1:
+    if columns % 128 or own % 8 or n_ep % 2 or n_tp % 2 or w_gate.shape[0] != 1:
         return shards(
             tokens,
             mix_gain,
@@ -502,11 +592,12 @@
         scratch_shapes=[pltpu.VMEM(a.shape, a.dtype) for a in operands]
         + [
             pltpu.VMEM((own, w_value.shape[1]), f32),
-            pltpu.VMEM((n_tp, own, width), bf16),
-            pltpu.VMEM((n_ep, own, width), bf16),
+            pltpu.VMEM((2, own, width // 2), bf16),
+            pltpu.VMEM((n_tp, own, width // 2), bf16),
+            pltpu.VMEM((2, n_ep, own, width // 2), bf16),
             pltpu.VMEM((n_ep, cap, columns), bf16),
-            pltpu.VMEM((n_ep, cap, columns), bf16),
-            pltpu.VMEM((n_tp, count, columns), bf16),
+            pltpu.VMEM((n_tp // 2, n_ep, cap, columns), bf16),
+            pltpu.VMEM((2, count, columns), bf16),
             dma((len(operands),)),
             dma((n_tp,)),
             dma((n_tp,)),
@@ -514,8 +605,10 @@
             dma((n_ep,)),
             dma((n_ep,)),
             dma((n_ep,)),
-            dma((n_tp,)),
-            dma((n_tp,)),
+            dma((n_tp // 2, n_ep)),
+            dma((n_tp // 2, n_ep)),
+            dma((2,)),
+            dma((2,)),
         ],
         compiler_params=pltpu.CompilerParams(
             collective_id=0, has_side_effects=True

time: 24.3 us -> 22.2 us (0.914)
  Pallas kernels: 23.4 us -> 21.3 us
    pallas_call x1, Pallas kernels: 22.4 us -> 20.3 us  [layer(): pl.pallas_call(functools.partial(layer_kernel, n_ep, n_tp, cap), out_shap...]
where the time goes in v4:
time: 22.2 us; the launch traced here: 22 us
  Pallas kernels  21.3 us (96%)
  between operations  0.65 us (3%)
    pallas_call x1, Pallas kernels, layer(): pl.pallas_call(functools.partial(layer_kernel, n_ep, n_tp, cap), out_shap...  20.3 us
    pallas_call x1, Pallas kernels, layer(): pl.pallas_call(write_results, out_shape=tuple((jax.ShapeDtypeStruct(*resu...  1.02 us

profile of v4, /device:TPU:0, one launch (start us, length us, event | category | flops | bytes accessed | tf_op | source)
XLA Modules:
  0.0 22.0 jit_solution(13778156521344036040)
XLA Ops:
  0.6 20.3 %shard_map.219 = (bf16[64,128]{1,0:T(8,128)(2,1)S(1)}, f32[8,128,256]{2,1,0:T(8,128)S(1)}, f32[8,1,128]{2,1,0:T(1,128)S(1)}, f32[1,8]{1,0:T(1,128)S(1)}) custom-call(bf16[8,1024]{1,0:T(8,128)(2,1)} %refs_0_.1, f32[1,1024]{1,0:T(1,128)} %bitcast.23, bf16[1024,128]{1,0:T(8,128)(2,1)} %refs_2_.1, bf16[1024,128]{1,0:T(8,128)(2,1)} %refs_3_.1, ...), custom_call_target="tpu_custom_call" | custom-call | tf_op jit(solution)/shard_map/pallas_call | solution.py:587
  20.9 1.0 %shard_map.220 = (bf16[64,128]{1,0:T(8,128)(2,1)}, f32[8,128,256]{2,1,0:T(8,128)}, f32[8,1,128]{2,1,0:T(1,128)}, f32[1,8]{1,0:T(1,128)}) custom-call(bf16[64,128]{1,0:T(8,128)(2,1)S(1)} %get-tuple-element.12.refs_0_, f32[8,128,256]{2,1,0:T(8,128)S(1)} %get-tuple-element.13.refs_1_, f32[8,1,128]{2,1,0:T(1,128)S(1)} %get-tuple-element.14.refs_2_, ...), custom_call_target="tpu_custom_call" | custom-call | tf_op jit(solution)/shard_map/pallas_call | solution.py:617
